TPU v7x, 32 devices: a whole 2x2x4 slice. The times are simulated.
32 devices in a mesh: sp: 4 (over z), dp: 8 (over y, x, core).
Axes of the slice: x: 2, y: 2, z: 4, core: 2. Of those that a mesh axis runs over, the one named last changes fastest.
Arguments:
- inputs: bfloat16 [8, 512, 2048], P('dp', 'sp'), may hold values from -6 to 6
- queries: bfloat16 [8, 512, 1024], P('dp', 'sp'), may hold values from -6 to 6
- keys: bfloat16 [8, 512, 1024], P('dp', 'sp'), may hold values from -1.5 to 1.5
- values: bfloat16 [8, 512, 1024], P('dp', 'sp'), may hold values from -6 to 6
- log_decay: bfloat16 [8, 512, 1024], P('dp', 'sp'), may hold values from -0.1 to 0, as said below
- cotangent: bfloat16 [8, 512, 1024], P('dp', 'sp'), may hold values from -0.59765625 to 0.59765625
- value_weight: bfloat16 [2048, 1024], P('dp'), may hold values from -0.125 to 0.125
Outputs:
- grad_queries: bfloat16 [8, 512, 1024], P('dp', 'sp')
- grad_keys: bfloat16 [8, 512, 1024], P('dp', 'sp')
- grad_decay: bfloat16 [8, 512, 1024], P('dp', 'sp')
- grad_inputs: bfloat16 [8, 512, 2048], P('dp', 'sp')
- grad_weight: float32 [2048, 1024], P('dp')
Inputs may be any that keep to these rules, and one draw needn't show every extreme that they name: `log_decay`: the log decays are negative; per key channel and sequence they differ between positions.
All inputs are finite; a program needn't handle non-finite values.
Results may differ from a plain program's by a relative error of at most 0.015.
Values may be sent and summed in bfloat16 or wider, within the bound.
A program may use at most 128 MiB of HBM per device.

v0:
```python
import functools

import jax
import jax.numpy as jnp
from jax import lax
from jax.experimental import pallas as pl
from jax.experimental.pallas import tpu as pltpu
from jax.sharding import PartitionSpec as P

HEAD_DIM = 64
PAIR = 128
BF = jnp.bfloat16
F32 = jnp.float32


def nt(a, b):
    return lax.dot_general(a, b, (((1,), (1,)), ((), ())), preferred_element_type=F32)


def nn(a, b):
    return lax.dot_general(a, b, (((1,), (0,)), ((), ())), preferred_element_type=F32)


def tn(a, b):
    return lax.dot_general(a, b, (((0,), (0,)), ((), ())), preferred_element_type=F32)


def split(a):
    hi = a.astype(BF)
    return hi, (a - hi.astype(F32)).astype(BF)


def kernel(
    sp, chips, chunks,
    x_ref, q_ref, k_ref, v_ref, g_ref, o_ref, w_ref,
    dq_ref, dk_ref, dg_ref, gi_ref, gw_ref,
    qf_s, kf_s, qb_s, kb_s, ke_s, qr_s,
    ec_s, en_s, ex_s, enx_s, eer_s,
    dqf_s, dqb_s, dkf_s, dkb_s, dv_s,
    sf_s, sb_s, ee_s,
    fin, bin_, fout, bout,
    xin, xt, vgs, wpair, gin, gout,
    half_out, half_in, part, gfin, gbin, gfout, gbout,
    s_f, r_f, s_b, r_b, s_x, r_x, s_v, r_v, s_w, r_w, s_g, r_g, s_h, r_h,
    s_gf, r_gf, s_gb, r_gb, loc,
):
    tokens, width = q_ref.shape
    pairs = width // PAIR
    rows = w_ref.shape[0]
    z = lax.axis_index("sp")
    d = lax.axis_index("dp")
    chip = d // 2
    core = lax.rem(d, 2)
    partner = chip * 2 + (1 - core)
    first = z == 0
    last = z == sp - 1
    inner = jnp.logical_and(z > 0, z < sp - 1)
    lower_half = z < sp // 2

    def peer(j):
        other = lax.rem(chip + j, chips)
        return other, other * 2 + core

    barrier = pltpu.get_barrier_semaphore()
    for j in range(1, chips):
        pl.semaphore_signal(barrier, inc=1, device_id={"dp": peer(j)[1]})
    pl.semaphore_signal(barrier, inc=1, device_id={"dp": partner})

    for step in (1, sp - 1):
        pl.semaphore_signal(barrier, inc=1, device_id={"sp": lax.rem(z + step, sp)})
    pl.semaphore_wait(barrier, chips + 2)

    def mine(i):
        return pl.ds(pl.multiple_of(i * tokens, tokens), tokens)

    def chip_cols(i):
        return pl.ds(pl.multiple_of(i * 2 * rows, 2 * rows), 2 * rows)

    def copy_x(j):
        other, idx = peer(j)
        return pltpu.make_async_remote_copy(
            x_ref.at[:, chip_cols(other)], xin.at[mine(chip)], s_x.at[j], r_x.at[j],
            device_id={"dp": idx})

    def copy_w():
        return pltpu.make_async_remote_copy(
            w_ref, wpair.at[pl.ds(pl.multiple_of(core * rows, rows), rows)], s_w, r_w,
            device_id={"dp": partner})

    def lanes(p):
        return pl.ds(pl.multiple_of(p * PAIR, PAIR), PAIR)

    def copy_v(j, p):
        _, idx = peer(j)
        return pltpu.make_async_remote_copy(
            vgs.at[mine(chip), lanes(p)], vgs.at[mine(chip), lanes(p)],
            s_v.at[j, p], r_v.at[j, p], device_id={"dp": idx})

    def copy_f(p):
        return pltpu.make_async_remote_copy(
            fout.at[p], fin.at[p], s_f.at[p], r_f.at[p], device_id={"sp": z + 1})

    def copy_b(p):
        return pltpu.make_async_remote_copy(
            bout.at[p], bin_.at[p], s_b.at[p], r_b.at[p], device_id={"sp": z - 1})

    for j in range(1, chips):
        copy_x(j).start()
    copy_w().start()
    own_x = pltpu.make_async_copy(x_ref.at[:, chip_cols(chip)], xin.at[mine(chip)], loc.at[0])
    own_x.start()
    own_w = pltpu.make_async_copy(
        w_ref, wpair.at[pl.ds(pl.multiple_of(core * rows, rows), rows)], loc.at[1])
    own_w.start()

    @pl.when(first)
    def _():
        fin[...] = jnp.zeros_like(fin)

    @pl.when(last)
    def _():
        bin_[...] = jnp.zeros_like(bin_)

    ti = lax.broadcasted_iota(jnp.int32, (tokens, tokens), 0)
    tj = lax.broadcasted_iota(jnp.int32, (tokens, tokens), 1)
    tril = jnp.where(tj <= ti, 1.0, 0.0).astype(BF)
    triu = jnp.where(tj >= ti, 1.0, 0.0).astype(BF)
    ci = lax.broadcasted_iota(jnp.int32, (PAIR, PAIR), 0)
    cj = lax.broadcasted_iota(jnp.int32, (PAIR, PAIR), 1)
    diag = (ci < HEAD_DIM) == (cj < HEAD_DIM)
    ones_c = jnp.ones((tokens, PAIR), BF)
    left = lax.broadcasted_iota(jnp.int32, (tokens, PAIR), 1) < HEAD_DIM
    ri = lax.broadcasted_iota(jnp.int32, (2 * tokens, tokens), 0)
    rj = lax.broadcasted_iota(jnp.int32, (2 * tokens, tokens), 1)
    rt = jnp.where(ri >= tokens, ri - tokens, ri)
    low2 = rt >= rj
    up2 = rt <= rj

    def stack(a):
        zero = jnp.zeros_like(a)
        return jnp.concatenate([jnp.where(left, a, zero), jnp.where(left, zero, a)], axis=0)

    def phase_a(p, carry):
        sl = lanes(p)
        gate = g_ref[:, sl]
        run = nn(tril, gate)
        excl = run - gate.astype(F32)
        ec = jnp.exp(run)
        en = jnp.exp(-run)
        ex = jnp.exp(excl)
        enx = jnp.exp(-excl)
        eer = ec[tokens - 1:tokens, :]
        qs = q_ref[:, sl].astype(F32) * HEAD_DIM ** (-0.5)
        ks = k_ref[:, sl].astype(F32)
        qf = (qs * ec).astype(BF)
        kb = (ks * ex).astype(BF)
        ke = (ks * (en * eer)).astype(BF)
        qr = (qs * (enx * eer)).astype(BF)
        qf_s[:, sl] = qf
        kf_s[:, sl] = (ks * en).astype(BF)
        qb_s[:, sl] = (qs * enx).astype(BF)
        kb_s[:, sl] = kb
        ke_s[:, sl] = ke
        qr_s[:, sl] = qr
        ec_s[:, sl] = ec
        en_s[:, sl] = en
        ex_s[:, sl] = ex
        enx_s[:, sl] = enx
        eer_s[:, sl] = jnp.broadcast_to(eer, (8, PAIR))
        val = v_ref[:, sl]
        cot = o_ref[:, sl]
        cot_r = pltpu.roll(cot.astype(F32), HEAD_DIM, 1).astype(BF)
        sf = jnp.where(diag, tn(ke, val), tn(qr, cot_r))
        sb = jnp.where(diag, tn(kb, val), tn(qf, cot_r))
        sf_s[p] = sf
        sb_s[p] = sb
        ee_s[p] = jnp.exp(tn(gate, ones_c))

        @pl.when(first)
        def _():
            fout[p] = sf.astype(BF)
            copy_f(p).start()

        @pl.when(last)
        def _():
            bout[p] = sb.astype(BF)
            copy_b(p).start()

        return carry

    lax.fori_loop(0, pairs, phase_a, 0)

    def forward_step(p):
        copy_f(p).wait_recv()

        @pl.when(z < sp - 1)
        def _():
            fout[p] = (ee_s[p] * fin[p].astype(F32) + sf_s[p]).astype(BF)
            copy_f(p).start()

    def backward_step(p):
        copy_b(p).wait_recv()

        @pl.when(z > 0)
        def _():
            bout[p] = (ee_s[p] * bin_[p].astype(F32) + sb_s[p]).astype(BF)
            copy_b(p).start()

    def phase_b(p, carry):
        sl = lanes(p)
        qf2 = stack(qf_s[:, sl])
        qb2 = stack(qb_s[:, sl])
        cot2 = stack(o_ref[:, sl])
        kf = kf_s[:, sl]
        kb = kb_s[:, sl]
        score = jnp.where(low2, nt(qf2, kf), 0.0) + jnp.where(up2, nt(qb2, kb), 0.0)
        dscore = nt(cot2, v_ref[:, sl])
        dlow = jnp.where(low2, dscore, 0.0).astype(BF)
        dup = jnp.where(up2, dscore, 0.0).astype(BF)
        dv_s[:, sl] = tn(score.astype(BF), cot2)
        dkf_s[:, sl] = tn(dlow, qf2)
        dkb_s[:, sl] = tn(dup, qb2)
        dqf_s[:, sl] = nn(jnp.concatenate([dlow[:tokens], dlow[tokens:]], axis=1), stack(kf))
        dqb_s[:, sl] = nn(jnp.concatenate([dup[:tokens], dup[tokens:]], axis=1), stack(kb))

        @pl.when(jnp.logical_and(lower_half, z > 0))
        def _():
            forward_step(p)

        @pl.when(jnp.logical_and(jnp.logical_not(lower_half), z < sp - 1))
        def _():
            backward_step(p)

        return carry

    lax.fori_loop(0, pairs, phase_b, 0)

    def phase_c(p, carry):
        sl = lanes(p)

        @pl.when(jnp.logical_and(lower_half, z < sp - 1))
        def _():
            backward_step(p)

        @pl.when(jnp.logical_and(jnp.logical_not(lower_half), z > 0))
        def _():
            forward_step(p)

        f_in = fin[p].astype(F32)
        b_in = bin_[p].astype(F32)
        b_roll = pltpu.roll(b_in, HEAD_DIM, 1)
        before = jnp.where(diag, f_in, 0.0).astype(BF)
        gb = jnp.where(diag, pltpu.roll(f_in, HEAD_DIM, 1), 0.0).astype(BF)
        after = jnp.where(diag, b_in, 0.0).astype(BF)
        gf = jnp.where(diag, b_roll, 0.0).astype(BF)
        val = v_ref[:, sl]
        cot = o_ref[:, sl]
        ke = ke_s[:, sl]
        kb = kb_s[:, sl]
        dv = dv_s[:, sl] + nn(ke, gf) + nn(kb, gb)
        vgs[mine(chip), sl] = dv.astype(BF)
        for j in range(1, chips):
            copy_v(j, p).start()
        dqf = dqf_s[:, sl] + nt(cot, before)
        dqr = nt(cot, after)
        dke = nt(val, gf)
        dkb = dkb_s[:, sl] + nt(val, gb)
        dqb = dqb_s[:, sl]
        dkf = dkf_s[:, sl]
        eer = eer_s[0:1, sl]
        enx = enx_s[:, sl]
        en = en_s[:, sl]
        dq_ref[:, sl] = (
            (dqf * ec_s[:, sl] + (dqb + dqr * eer) * enx) * HEAD_DIM ** (-0.5)
        ).astype(BF)
        dk_ref[:, sl] = ((dkf + dke * eer) * en + dkb * ex_s[:, sl]).astype(BF)
        u1 = (
            qf_s[:, sl].astype(F32) * dqf
            - kf_s[:, sl].astype(F32) * dkf
            - ke.astype(F32) * dke
        )
        u2 = (
            kb.astype(F32) * dkb
            - qb_s[:, sl].astype(F32) * dqb
            - qr_s[:, sl].astype(F32) * dqr
        )
        cross = (ee_s[p] * f_in + sf_s[p]) * b_roll
        u_hi, u_lo = split(u1 + u2)
        c_hi, c_lo = split(cross)
        dg_ref[:, sl] = (
            nn(triu, u_hi) + nn(triu, u_lo) + nt(ones_c, c_hi) + nt(ones_c, c_lo) - u2
        ).astype(BF)
        return carry

    lax.fori_loop(0, pairs, phase_c, 0)

    own_x.wait()
    own_w.wait()
    copy_w().wait()
    for j in range(1, chips):
        copy_x(j).wait()
    xt[...] = jnp.transpose(xin[...])

    def wait_v(p, carry):
        for j in range(1, chips):
            copy_v(j, p).wait()
        return carry

    lax.fori_loop(0, pairs, wait_v, 0)

    def copy_h(c):
        return pltpu.make_async_remote_copy(
            half_out.at[c], half_in.at[c], s_h.at[c], r_h.at[c], device_id={"dp": partner})

    size = rows // chunks

    def product(side, c):
        at = pl.ds(pl.multiple_of(side * rows + c * size, size), size)
        return nn(xt[at, :], vgs[...])

    for c in range(chunks):
        half_out[c] = product(1 - core, c).astype(BF)
        copy_h(c).start()
    for c in range(chunks):
        part[c] = product(core, c)

    def copy_gf(c):
        return pltpu.make_async_remote_copy(
            gfout.at[c], gfin.at[c], s_gf.at[c], r_gf.at[c], device_id={"sp": z + 1})

    def copy_gb(c):
        return pltpu.make_async_remote_copy(
            gbout.at[c], gbin.at[c], s_gb.at[c], r_gb.at[c], device_id={"sp": z - 1})

    for c in range(chunks):
        copy_h(c).wait()
        total = part[c] + half_in[c].astype(F32)
        part[c] = total

        @pl.when(first)
        def _():
            gfout[c] = total.astype(BF)
            copy_gf(c).start()

        @pl.when(last)
        def _():
            gbout[c] = total.astype(BF)
            copy_gb(c).start()

    def sum_forward(c):
        copy_gf(c).wait_recv()

        @pl.when(z < sp - 1)
        def _():
            gfout[c] = (part[c] + gfin[c].astype(F32)).astype(BF)
            copy_gf(c).start()

    def sum_backward(c):
        copy_gb(c).wait_recv()

        @pl.when(z > 0)
        def _():
            gbout[c] = (part[c] + gbin[c].astype(F32)).astype(BF)
            copy_gb(c).start()

    @pl.when(jnp.logical_and(lower_half, z > 0))
    def _():
        for c in range(chunks):
            sum_forward(c)

    @pl.when(jnp.logical_and(jnp.logical_not(lower_half), z < sp - 1))
    def _():
        for c in range(chunks):
            sum_backward(c)

    def copy_g(j):
        other, idx = peer(j)
        return pltpu.make_async_remote_copy(
            gout.at[mine(other)], gin.at[chip], s_g.at[j], r_g.at[j], device_id={"dp": idx})

    def project(j):
        other, _ = peer(j)
        gout[mine(other), :] = nt(vgs[mine(other), :], wpair[...]).astype(BF)

    for j in range(1, chips):
        project(j)
        copy_g(j).start()
    project(0)
    gi_ref[:, chip_cols(chip)] = gout[mine(chip), :]

    @pl.when(jnp.logical_and(lower_half, z < sp - 1))
    def _():
        for c in range(chunks):
            sum_backward(c)

    @pl.when(jnp.logical_and(jnp.logical_not(lower_half), z > 0))
    def _():
        for c in range(chunks):
            sum_forward(c)

    for c in range(chunks):
        gw_ref[pl.ds(c * size, size), :] = part[c]

    @pl.when(z > 0)
    def _():
        for c in range(chunks):
            gw_ref[pl.ds(c * size, size), :] += gfin[c].astype(F32)

    @pl.when(z < sp - 1)
    def _():
        for c in range(chunks):
            gw_ref[pl.ds(c * size, size), :] += gbin[c].astype(F32)

    for j in range(1, chips):
        copy_g(j).wait()
    for j in range(1, chips):
        other, _ = peer(j)
        gi_ref[:, chip_cols(other)] = gin[other]

    @pl.when(z < sp - 1)
    def _():
        for c in range(chunks):
            copy_gf(c).wait_send()

        def drain(p, carry):
            copy_f(p).wait_send()
            return carry

        lax.fori_loop(0, pairs, drain, 0)

    @pl.when(z > 0)
    def _():
        for c in range(chunks):
            copy_gb(c).wait_send()

        def drain(p, carry):
            copy_b(p).wait_send()
            return carry

        lax.fori_loop(0, pairs, drain, 0)


def per_device(sp, dp, inputs, queries, keys, values, log_decay, cotangent, value_weight):
    tokens, model = inputs.shape[1:]
    width = queries.shape[2]
    rows = value_weight.shape[0]
    chips = dp // 2
    pairs = width // PAIR
    chunks = 4
    size = rows // chunks
    wide = lambda t: pltpu.VMEM((tokens, width), t)
    state = lambda t: pltpu.VMEM((pairs, PAIR, PAIR), t)
    dma = lambda *n: pltpu.SemaphoreType.DMA(n)
    piece = lambda t: pltpu.VMEM((chunks, size, width), t)
    outs = pl.pallas_call(
        functools.partial(kernel, sp, chips, chunks),
        out_shape=[jax.ShapeDtypeStruct((tokens, width), BF)] * 3
        + [jax.ShapeDtypeStruct((tokens, model), BF), jax.ShapeDtypeStruct((rows, width), F32)],
        in_specs=[pl.BlockSpec(memory_space=pltpu.VMEM)] * 7,
        out_specs=[pl.BlockSpec(memory_space=pltpu.VMEM)] * 5,
        scratch_shapes=[wide(BF)] * 6
        + [wide(F32)] * 4
        + [pltpu.VMEM((8, width), F32)]
        + [wide(F32)] * 5
        + [state(F32)] * 3
        + [state(BF)] * 4
        + [
            pltpu.VMEM((chips * tokens, 2 * rows), BF),
            pltpu.VMEM((2 * rows, chips * tokens), BF),
            pltpu.VMEM((chips * tokens, width), BF),
            pltpu.VMEM((2 * rows, width), BF),
            pltpu.VMEM((chips, tokens, 2 * rows), BF),
            pltpu.VMEM((chips * tokens, 2 * rows), BF),
            piece(BF), piece(BF), piece(F32), piece(BF), piece(BF), piece(BF), piece(BF),
        ]
        + [dma(pairs)] * 4
        + [dma(chips)] * 2
        + [dma(chips, pairs)] * 2
        + [pltpu.SemaphoreType.DMA] * 2
        + [dma(chips)] * 2
        + [dma(chunks)] * 6
        + [dma(2)],
        compiler_params=pltpu.CompilerParams(
            collective_id=0, has_side_effects=True, vmem_limit_bytes=60 * 1024 * 1024),
    )(inputs[0], queries[0], keys[0], values[0], log_decay[0], cotangent[0], value_weight)
    return outs[0][None], outs[1][None], outs[2][None], outs[3][None], outs[4]


def solution(mesh):
    row = P("dp", "sp", None)
    return jax.shard_map(
        functools.partial(per_device, mesh.shape["sp"], mesh.shape["dp"]),
        mesh=mesh,
        in_specs=(row,) * 6 + (P("dp", None),),
        out_specs=(row,) * 4 + (P("dp", None),),
        check_vma=False,
    )
```

profile of v0, /device:TPU:0, one launch (start us, length us, event | category | flops | bytes accessed | tf_op | source)
XLA Modules:
  0.0 68.1 jit_solution(4362090205604808935)
XLA Ops:
  0.6 62.5 %shard_map.110 = (bf16[128,1024]{1,0:T(8,128)(2,1)}, bf16[128,1024]{1,0:T(8,128)(2,1)}, bf16[128,1024]{1,0:T(8,128)(2,1)}, bf16[128,2048]{1,0:T(8,128)(2,1)}, f32[256,1024]{1,0:T(8,128)}) custom-call(bf16[128,2048]{1,0:T(8,128)(2,1)} %bitcast.11, bf16[128,1024]{1,0:T(8,128)(2,1)} %bitcast.12, bf16[128,1024]{1,0:T(8,128)(2,1)} %bitcast.13, ...), custom_call_target="tpu_custom_call" | custom-call | tf_op jit(solution)/shard_map/pallas_call | solution.py:455
  63.1 0.0 copy-start.3
  63.1 0.0 copy-start.2
  63.1 0.0 copy-start.1
  63.2 1.8 %copy.17 = bf16[1,128,1024]{2,1,0:T(8,128)(2,1)} copy(bf16[1,128,1024]{2,1,0:T(8,128)(2,1)} %bitcast.19) | data formatting | bytes 524288
  64.9 0.0 copy-done.3
  64.9 0.0 copy-start
  64.9 0.7 %copy.18 = bf16[1,128,1024]{2,1,0:T(8,128)(2,1)} copy(bf16[1,128,1024]{2,1,0:T(8,128)(2,1)S(1)} %bitcast.18) | data formatting | bytes 524288
  65.6 0.0 copy-done.2
  65.6 0.7 %copy.19 = bf16[1,128,1024]{2,1,0:T(8,128)(2,1)} copy(bf16[1,128,1024]{2,1,0:T(8,128)(2,1)S(1)} %bitcast.17) | data formatting | bytes 524288
  66.3 0.0 copy-done.1
  66.3 0.8 %copy.20 = bf16[1,128,2048]{2,1,0:T(8,128)(2,1)} copy(bf16[1,128,2048]{2,1,0:T(8,128)(2,1)S(1)} %bitcast.10) | data formatting | bytes 1048576
  67.1 0.0 copy-done
  67.1 1.0 %copy.21 = f32[256,1024]{1,0:T(8,128)} copy(f32[256,1024]{1,0:T(8,128)S(1)} %copy-done) | data formatting | bytes 2097152
Async XLA Ops:
  63.1 1.8 %copy-start.3 = (bf16[128,1024]{1,0:T(8,128)(2,1)S(1)}, bf16[128,1024]{1,0:T(8,128)(2,1)}, u32[]{:S(2)}) copy-start(bf16[128,1024]{1,0:T(8,128)(2,1)} %get-tuple-element.11) | copy-start | bytes 786436
  63.1 2.5 %copy-start.2 = (bf16[128,1024]{1,0:T(8,128)(2,1)S(1)}, bf16[128,1024]{1,0:T(8,128)(2,1)}, u32[]{:S(2)}) copy-start(bf16[128,1024]{1,0:T(8,128)(2,1)} %get-tuple-element.12) | copy-start | bytes 786436
  63.1 3.2 %copy-start.1 = (bf16[128,2048]{1,0:T(8,128)(2,1)S(1)}, bf16[128,2048]{1,0:T(8,128)(2,1)}, u32[]{:S(2)}) copy-start(bf16[128,2048]{1,0:T(8,128)(2,1)} %get-tuple-element.13) | copy-start | bytes 1572868
  64.9 2.2 %copy-start = (f32[256,1024]{1,0:T(8,128)S(1)}, f32[256,1024]{1,0:T(8,128)}, u32[]{:S(2)}) copy-start(f32[256,1024]{1,0:T(8,128)} %get-tuple-element.24) | copy-start | bytes 3145732
where the time goes:
time: 68.3 us; the launch traced here: 68.1 us
  Pallas kernels  62.5 us (92%)
  local copies, waits for them, and re-layouts  4.94 us (7%)
    pallas_call x1, Pallas kernels, per_device(): pl.pallas_call(functools.partial(kernel, sp, chips, chunks), out_shape=[j...  62.5 us
    unnamed x13, local copies, waits for them, and re-layouts  4.94 us

commit v1 on v0

--- a/solution.py
+++ b/solution.py
@@ -31,7 +31,7 @@
 
 
 def kernel(
-    sp, chips, chunks,
+    sp, chips,
     x_ref, q_ref, k_ref, v_ref, g_ref, o_ref, w_ref,
     dq_ref, dk_ref, dg_ref, gi_ref, gw_ref,
     qf_s, kf_s, qb_s, kb_s, ke_s, qr_s,
@@ -68,8 +68,6 @@
 
     for step in (1, sp - 1):
         pl.semaphore_signal(barrier, inc=1, device_id={"sp": lax.rem(z + step, sp)})
-    pl.semaphore_wait(barrier, chips + 2)
-
     def mine(i):
         return pl.ds(pl.multiple_of(i * tokens, tokens), tokens)
 
@@ -103,6 +101,8 @@
     def copy_b(p):
         return pltpu.make_async_remote_copy(
             bout.at[p], bin_.at[p], s_b.at[p], r_b.at[p], device_id={"sp": z - 1})
+
+    pl.semaphore_wait(barrier, chips + 2)
 
     for j in range(1, chips):
         copy_x(j).start()
@@ -116,10 +116,12 @@
     @pl.when(first)
     def _():
         fin[...] = jnp.zeros_like(fin)
+        gfin[...] = jnp.zeros_like(gfin)
 
     @pl.when(last)
     def _():
         bin_[...] = jnp.zeros_like(bin_)
+        gbin[...] = jnp.zeros_like(gbin)
 
     ti = lax.broadcasted_iota(jnp.int32, (tokens, tokens), 0)
     tj = lax.broadcasted_iota(jnp.int32, (tokens, tokens), 1)
@@ -206,6 +208,17 @@
             bout[p] = (ee_s[p] * bin_[p].astype(F32) + sb_s[p]).astype(BF)
             copy_b(p).start()
 
+    lag = pairs // 2
+
+    def second_step(p, gate):
+        @pl.when(jnp.logical_and(gate, jnp.logical_and(lower_half, z < sp - 1)))
+        def _():
+            backward_step(p)
+
+        @pl.when(jnp.logical_and(gate, jnp.logical_and(jnp.logical_not(lower_half), z > 0)))
+        def _():
+            forward_step(p)
+
     def phase_b(p, carry):
         sl = lanes(p)
         qf2 = stack(qf_s[:, sl])
@@ -231,36 +244,40 @@
         def _():
             backward_step(p)
 
+        second_step(p - lag, jnp.logical_and(inner, p >= lag))
         return carry
 
     lax.fori_loop(0, pairs, phase_b, 0)
 
-    def phase_c(p, carry):
+    def received(p):
+        f_in = fin[p].astype(F32)
+        b_roll = pltpu.roll(bin_[p].astype(F32), HEAD_DIM, 1)
+        gb = jnp.where(diag, pltpu.roll(f_in, HEAD_DIM, 1), 0.0).astype(BF)
+        gf = jnp.where(diag, b_roll, 0.0).astype(BF)
+        return f_in, b_roll, gb, gf
+
+    def phase_v(p, carry):
         sl = lanes(p)
-
-        @pl.when(jnp.logical_and(lower_half, z < sp - 1))
-        def _():
-            backward_step(p)
-
-        @pl.when(jnp.logical_and(jnp.logical_not(lower_half), z > 0))
-        def _():
-            forward_step(p)
-
-        f_in = fin[p].astype(F32)
-        b_in = bin_[p].astype(F32)
-        b_roll = pltpu.roll(b_in, HEAD_DIM, 1)
+        second_step(p, jnp.logical_not(inner))
+        second_step(p + lag, jnp.logical_and(inner, p < pairs - lag))
+        _, _, gb, gf = received(p)
+        dv = dv_s[:, sl] + nn(ke_s[:, sl], gf) + nn(kb_s[:, sl], gb)
+        vgs[mine(chip), sl] = dv.astype(BF)
+        for j in range(1, chips):
+            copy_v(j, p).start()
+        return carry
+
+    lax.fori_loop(0, pairs, phase_v, 0)
+
+    def phase_c(p):
+        sl = lanes(p)
+        f_in, b_roll, gb, gf = received(p)
         before = jnp.where(diag, f_in, 0.0).astype(BF)
-        gb = jnp.where(diag, pltpu.roll(f_in, HEAD_DIM, 1), 0.0).astype(BF)
-        after = jnp.where(diag, b_in, 0.0).astype(BF)
-        gf = jnp.where(diag, b_roll, 0.0).astype(BF)
+        after = jnp.where(diag, bin_[p].astype(F32), 0.0).astype(BF)
         val = v_ref[:, sl]
         cot = o_ref[:, sl]
         ke = ke_s[:, sl]
         kb = kb_s[:, sl]
-        dv = dv_s[:, sl] + nn(ke, gf) + nn(kb, gb)
-        vgs[mine(chip), sl] = dv.astype(BF)
-        for j in range(1, chips):
-            copy_v(j, p).start()
         dqf = dqf_s[:, sl] + nt(cot, before)
         dqr = nt(cot, after)
         dke = nt(val, gf)
@@ -290,9 +307,6 @@
         dg_ref[:, sl] = (
             nn(triu, u_hi) + nn(triu, u_lo) + nt(ones_c, c_hi) + nt(ones_c, c_lo) - u2
         ).astype(BF)
-        return carry
-
-    lax.fori_loop(0, pairs, phase_c, 0)
 
     own_x.wait()
     own_w.wait()
@@ -301,77 +315,86 @@
         copy_x(j).wait()
     xt[...] = jnp.transpose(xin[...])
 
-    def wait_v(p, carry):
+    def copy_h(p):
+        return pltpu.make_async_remote_copy(
+            half_out.at[p], half_in.at[p], s_h.at[p], r_h.at[p], device_id={"dp": partner})
+
+    def copy_gf(p):
+        return pltpu.make_async_remote_copy(
+            gfout.at[p], gfin.at[p], s_gf.at[p], r_gf.at[p], device_id={"sp": z + 1})
+
+    def copy_gb(p):
+        return pltpu.make_async_remote_copy(
+            gbout.at[p], gbin.at[p], s_gb.at[p], r_gb.at[p], device_id={"sp": z - 1})
+
+    def product(side, p):
+        at = pl.ds(pl.multiple_of(side * rows, rows), rows)
+        return nn(xt[at, :], vgs[:, lanes(p)])
+
+    def make_term(p):
         for j in range(1, chips):
             copy_v(j, p).wait()
+        half_out[p] = product(1 - core, p).astype(BF)
+        copy_h(p).start()
+        part[p] = product(core, p)
+
+    def join(p):
+        copy_h(p).wait()
+        total = part[p] + half_in[p].astype(F32)
+        part[p] = total
+
+        @pl.when(first)
+        def _():
+            gfout[p] = total.astype(BF)
+            copy_gf(p).start()
+
+        @pl.when(last)
+        def _():
+            gbout[p] = total.astype(BF)
+            copy_gb(p).start()
+
+    def sum_forward(p):
+        copy_gf(p).wait_recv()
+
+        @pl.when(z < sp - 1)
+        def _():
+            gfout[p] = (part[p] + gfin[p].astype(F32)).astype(BF)
+            copy_gf(p).start()
+
+    def sum_backward(p):
+        copy_gb(p).wait_recv()
+
+        @pl.when(z > 0)
+        def _():
+            gbout[p] = (part[p] + gbin[p].astype(F32)).astype(BF)
+            copy_gb(p).start()
+
+    def sum_step(p, lower, upper):
+        within = jnp.logical_and(inner, jnp.logical_and(p >= 0, p < pairs))
+
+        @pl.when(jnp.logical_and(within, lower_half))
+        def _():
+            lower(p)
+
+        @pl.when(jnp.logical_and(within, jnp.logical_not(lower_half)))
+        def _():
+            upper(p)
+
+    def pipeline(i, carry):
+        @pl.when(i < pairs)
+        def _():
+            make_term(i)
+            phase_c(i)
+
+        @pl.when(jnp.logical_and(i >= 1, i <= pairs))
+        def _():
+            join(i - 1)
+
+        sum_step(i - 3, sum_forward, sum_backward)
+        sum_step(i - 5, sum_backward, sum_forward)
         return carry
 
-    lax.fori_loop(0, pairs, wait_v, 0)
-
-    def copy_h(c):
-        return pltpu.make_async_remote_copy(
-            half_out.at[c], half_in.at[c], s_h.at[c], r_h.at[c], device_id={"dp": partner})
-
-    size = rows // chunks
-
-    def product(side, c):
-        at = pl.ds(pl.multiple_of(side * rows + c * size, size), size)
-        return nn(xt[at, :], vgs[...])
-
-    for c in range(chunks):
-        half_out[c] = product(1 - core, c).astype(BF)
-        copy_h(c).start()
-    for c in range(chunks):
-        part[c] = product(core, c)
-
-    def copy_gf(c):
-        return pltpu.make_async_remote_copy(
-            gfout.at[c], gfin.at[c], s_gf.at[c], r_gf.at[c], device_id={"sp": z + 1})
-
-    def copy_gb(c):
-        return pltpu.make_async_remote_copy(
-            gbout.at[c], gbin.at[c], s_gb.at[c], r_gb.at[c], device_id={"sp": z - 1})
-
-    for c in range(chunks):
-        copy_h(c).wait()
-        total = part[c] + half_in[c].astype(F32)
-        part[c] = total
-
-        @pl.when(first)
-        def _():
-            gfout[c] = total.astype(BF)
-            copy_gf(c).start()
-
-        @pl.when(last)
-        def _():
-            gbout[c] = total.astype(BF)
-            copy_gb(c).start()
-
-    def sum_forward(c):
-        copy_gf(c).wait_recv()
-
-        @pl.when(z < sp - 1)
-        def _():
-            gfout[c] = (part[c] + gfin[c].astype(F32)).astype(BF)
-            copy_gf(c).start()
-
-    def sum_backward(c):
-        copy_gb(c).wait_recv()
-
-        @pl.when(z > 0)
-        def _():
-            gbout[c] = (part[c] + gbin[c].astype(F32)).astype(BF)
-            copy_gb(c).start()
-
-    @pl.when(jnp.logical_and(lower_half, z > 0))
-    def _():
-        for c in range(chunks):
-            sum_forward(c)
-
-    @pl.when(jnp.logical_and(jnp.logical_not(lower_half), z < sp - 1))
-    def _():
-        for c in range(chunks):
-            sum_backward(c)
+    lax.fori_loop(0, pairs + 1, pipeline, 0)
 
     def copy_g(j):
         other, idx = peer(j)
@@ -388,28 +411,22 @@
     project(0)
     gi_ref[:, chip_cols(chip)] = gout[mine(chip), :]
 
-    @pl.when(jnp.logical_and(lower_half, z < sp - 1))
-    def _():
-        for c in range(chunks):
-            sum_backward(c)
-
-    @pl.when(jnp.logical_and(jnp.logical_not(lower_half), z > 0))
-    def _():
-        for c in range(chunks):
-            sum_forward(c)
-
-    for c in range(chunks):
-        gw_ref[pl.ds(c * size, size), :] = part[c]
-
-    @pl.when(z > 0)
-    def _():
-        for c in range(chunks):
-            gw_ref[pl.ds(c * size, size), :] += gfin[c].astype(F32)
-
-    @pl.when(z < sp - 1)
-    def _():
-        for c in range(chunks):
-            gw_ref[pl.ds(c * size, size), :] += gbin[c].astype(F32)
+
+    lax.fori_loop(pairs + 1, pairs + 5, pipeline, 0)
+
+    def finish(p, carry):
+        @pl.when(first)
+        def _():
+            sum_backward(p)
+
+        @pl.when(last)
+        def _():
+            sum_forward(p)
+
+        gw_ref[:, lanes(p)] = part[p] + gfin[p].astype(F32) + gbin[p].astype(F32)
+        return carry
+
+    lax.fori_loop(0, pairs, finish, 0)
 
     for j in range(1, chips):
         copy_g(j).wait()
@@ -419,10 +436,8 @@
 
     @pl.when(z < sp - 1)
     def _():
-        for c in range(chunks):
-            copy_gf(c).wait_send()
-
         def drain(p, carry):
+            copy_gf(p).wait_send()
             copy_f(p).wait_send()
             return carry
 
@@ -430,10 +445,8 @@
 
     @pl.when(z > 0)
     def _():
-        for c in range(chunks):
-            copy_gb(c).wait_send()
-
         def drain(p, carry):
+            copy_gb(p).wait_send()
             copy_b(p).wait_send()
             return carry
 
@@ -446,14 +459,12 @@
     rows = value_weight.shape[0]
     chips = dp // 2
     pairs = width // PAIR
-    chunks = 4
-    size = rows // chunks
     wide = lambda t: pltpu.VMEM((tokens, width), t)
     state = lambda t: pltpu.VMEM((pairs, PAIR, PAIR), t)
     dma = lambda *n: pltpu.SemaphoreType.DMA(n)
-    piece = lambda t: pltpu.VMEM((chunks, size, width), t)
+    piece = lambda t: pltpu.VMEM((pairs, rows, PAIR), t)
     outs = pl.pallas_call(
-        functools.partial(kernel, sp, chips, chunks),
+        functools.partial(kernel, sp, chips),
         out_shape=[jax.ShapeDtypeStruct((tokens, width), BF)] * 3
         + [jax.ShapeDtypeStruct((tokens, model), BF), jax.ShapeDtypeStruct((rows, width), F32)],
         in_specs=[pl.BlockSpec(memory_space=pltpu.VMEM)] * 7,
@@ -478,7 +489,7 @@
         + [dma(chips, pairs)] * 2
         + [pltpu.SemaphoreType.DMA] * 2
         + [dma(chips)] * 2
-        + [dma(chunks)] * 6
+        + [dma(pairs)] * 6
         + [dma(2)],
         compiler_params=pltpu.CompilerParams(
             collective_id=0, has_side_effects=True, vmem_limit_bytes=60 * 1024 * 1024),

time: 68.3 us -> 54.5 us (0.80)
  Pallas kernels: 62.5 us -> 48.8 us
    pallas_call x1, Pallas kernels: 62.5 us -> 48.8 us  [per_device(): pl.pallas_call(functools.partial(kernel, sp, chips), out_shape=[jax.Shape...]
where the time goes in v1:
time: 54.5 us; the launch traced here: 54.4 us
  Pallas kernels  48.8 us (90%)
  local copies, waits for them, and re-layouts  4.94 us (9%)
  between operations  0.67 us (1%)
    pallas_call x1, Pallas kernels, per_device(): pl.pallas_call(functools.partial(kernel, sp, chips), out_shape=[jax.Shape...  48.8 us
    unnamed x13, local copies, waits for them, and re-layouts  4.94 us

profile of v1, /device:TPU:0, one launch (start us, length us, event | category | flops | bytes accessed | tf_op | source)
XLA Modules:
  0.0 54.4 jit_solution(4047506704176249484)
XLA Ops:
  0.6 48.8 %shard_map.110 = (bf16[128,1024]{1,0:T(8,128)(2,1)}, bf16[128,1024]{1,0:T(8,128)(2,1)}, bf16[128,1024]{1,0:T(8,128)(2,1)}, bf16[128,2048]{1,0:T(8,128)(2,1)}, f32[256,1024]{1,0:T(8,128)}) custom-call(bf16[128,2048]{1,0:T(8,128)(2,1)} %bitcast.11, bf16[128,1024]{1,0:T(8,128)(2,1)} %bitcast.12, bf16[128,1024]{1,0:T(8,128)(2,1)} %bitcast.13, ...), custom_call_target="tpu_custom_call" | custom-call | tf_op jit(solution)/shard_map/pallas_call | solution.py:466
  49.4 0.0 copy-start.3
  49.4 0.0 copy-start.2
  49.4 0.0 copy-start.1
  49.4 1.8 %copy.17 = bf16[1,128,1024]{2,1,0:T(8,128)(2,1)} copy(bf16[1,128,1024]{2,1,0:T(8,128)(2,1)} %bitcast.19) | data formatting | bytes 524288
  51.2 0.0 copy-done.3
  51.2 0.0 copy-start
  51.2 0.7 %copy.18 = bf16[1,128,1024]{2,1,0:T(8,128)(2,1)} copy(bf16[1,128,1024]{2,1,0:T(8,128)(2,1)S(1)} %bitcast.18) | data formatting | bytes 524288
  51.9 0.0 copy-done.2
  51.9 0.7 %copy.19 = bf16[1,128,1024]{2,1,0:T(8,128)(2,1)} copy(bf16[1,128,1024]{2,1,0:T(8,128)(2,1)S(1)} %bitcast.17) | data formatting | bytes 524288
  52.6 0.0 copy-done.1
  52.6 0.8 %copy.20 = bf16[1,128,2048]{2,1,0:T(8,128)(2,1)} copy(bf16[1,128,2048]{2,1,0:T(8,128)(2,1)S(1)} %bitcast.10) | data formatting | bytes 1048576
  53.4 0.0 copy-done
  53.4 1.0 %copy.21 = f32[256,1024]{1,0:T(8,128)} copy(f32[256,1024]{1,0:T(8,128)S(1)} %copy-done) | data formatting | bytes 2097152
Async XLA Ops:
  49.4 1.8 %copy-start.3 = (bf16[128,1024]{1,0:T(8,128)(2,1)S(1)}, bf16[128,1024]{1,0:T(8,128)(2,1)}, u32[]{:S(2)}) copy-start(bf16[128,1024]{1,0:T(8,128)(2,1)} %get-tuple-element.11) | copy-start | bytes 786436
  49.4 2.5 %copy-start.2 = (bf16[128,1024]{1,0:T(8,128)(2,1)S(1)}, bf16[128,1024]{1,0:T(8,128)(2,1)}, u32[]{:S(2)}) copy-start(bf16[128,1024]{1,0:T(8,128)(2,1)} %get-tuple-element.12) | copy-start | bytes 786436
  49.4 3.2 %copy-start.1 = (bf16[128,2048]{1,0:T(8,128)(2,1)S(1)}, bf16[128,2048]{1,0:T(8,128)(2,1)}, u32[]{:S(2)}) copy-start(bf16[128,2048]{1,0:T(8,128)(2,1)} %get-tuple-element.13) | copy-start | bytes 1572868
  51.2 2.2 %copy-start = (f32[256,1024]{1,0:T(8,128)S(1)}, f32[256,1024]{1,0:T(8,128)}, u32[]{:S(2)}) copy-start(f32[256,1024]{1,0:T(8,128)} %get-tuple-element.24) | copy-start | bytes 3145732

commit v2 on v1

--- a/solution.py
+++ b/solution.py
@@ -9,6 +9,7 @@
 
 HEAD_DIM = 64
 PAIR = 128
+VMEM_BYTES = 67043328
 BF = jnp.bfloat16
 F32 = jnp.float32
 
@@ -32,8 +33,9 @@
 
 def kernel(
     sp, chips,
-    x_ref, q_ref, k_ref, v_ref, g_ref, o_ref, w_ref,
+    x_ref, q_in, k_in, v_in, g_in, o_in, w_ref,
     dq_ref, dk_ref, dg_ref, gi_ref, gw_ref,
+    q_ref, k_ref, v_ref, g_ref, o_ref,
     qf_s, kf_s, qb_s, kb_s, ke_s, qr_s,
     ec_s, en_s, ex_s, enx_s, eer_s,
     dqf_s, dqb_s, dkf_s, dkb_s, dv_s,
@@ -57,6 +59,14 @@
     inner = jnp.logical_and(z > 0, z < sp - 1)
     lower_half = z < sp // 2
 
+    loads = [
+        pltpu.make_async_copy(a, b, loc.at[2 + i])
+        for i, (a, b) in enumerate(
+            ((g_in, g_ref), (q_in, q_ref), (k_in, k_ref), (v_in, v_ref), (o_in, o_ref)))
+    ]
+    for load in loads:
+        load.start()
+
     def peer(j):
         other = lax.rem(chip + j, chips)
         return other, other * 2 + core
@@ -112,6 +122,8 @@
     own_w = pltpu.make_async_copy(
         w_ref, wpair.at[pl.ds(pl.multiple_of(core * rows, rows), rows)], loc.at[1])
     own_w.start()
+    for load in loads:
+        load.wait()
 
     @pl.when(first)
     def _():
@@ -453,6 +465,17 @@
         lax.fori_loop(0, pairs, drain, 0)
 
 
+def write_out(*refs):
+    sems = refs[10]
+    copies = [
+        pltpu.make_async_copy(refs[i], refs[5 + i], sems.at[i]) for i in (4, 3, 0, 1, 2)
+    ]
+    for copy in copies:
+        copy.start()
+    for copy in copies:
+        copy.wait()
+
+
 def per_device(sp, dp, inputs, queries, keys, values, log_decay, cotangent, value_weight):
     tokens, model = inputs.shape[1:]
     width = queries.shape[2]
@@ -463,13 +486,15 @@
     state = lambda t: pltpu.VMEM((pairs, PAIR, PAIR), t)
     dma = lambda *n: pltpu.SemaphoreType.DMA(n)
     piece = lambda t: pltpu.VMEM((pairs, rows, PAIR), t)
+    shapes = [jax.ShapeDtypeStruct((tokens, width), BF)] * 3
+    shapes += [jax.ShapeDtypeStruct((tokens, model), BF), jax.ShapeDtypeStruct((rows, width), F32)]
+    kept = sum(a.size * a.dtype.itemsize for a in shapes) + 64 * 1024
     outs = pl.pallas_call(
         functools.partial(kernel, sp, chips),
-        out_shape=[jax.ShapeDtypeStruct((tokens, width), BF)] * 3
-        + [jax.ShapeDtypeStruct((tokens, model), BF), jax.ShapeDtypeStruct((rows, width), F32)],
-        in_specs=[pl.BlockSpec(memory_space=pltpu.VMEM)] * 7,
+        out_shape=[pltpu.VMEM(a.shape, a.dtype) for a in shapes],
+        in_specs=[pl.BlockSpec(memory_space=pltpu.MemorySpace.HBM)] * 7,
         out_specs=[pl.BlockSpec(memory_space=pltpu.VMEM)] * 5,
-        scratch_shapes=[wide(BF)] * 6
+        scratch_shapes=[wide(BF)] * 11
         + [wide(F32)] * 4
         + [pltpu.VMEM((8, width), F32)]
         + [wide(F32)] * 5
@@ -490,10 +515,18 @@
         + [pltpu.SemaphoreType.DMA] * 2
         + [dma(chips)] * 2
         + [dma(pairs)] * 6
-        + [dma(2)],
+        + [dma(7)],
         compiler_params=pltpu.CompilerParams(
-            collective_id=0, has_side_effects=True, vmem_limit_bytes=60 * 1024 * 1024),
+            collective_id=0, has_side_effects=True, vmem_limit_bytes=VMEM_BYTES - kept),
     )(inputs[0], queries[0], keys[0], values[0], log_decay[0], cotangent[0], value_weight)
+    outs = pl.pallas_call(
+        write_out,
+        out_shape=shapes,
+        in_specs=[pl.BlockSpec(memory_space=pl.ANY)] * 5,
+        out_specs=[pl.BlockSpec(memory_space=pl.ANY)] * 5,
+        scratch_shapes=[dma(5)],
+        compiler_params=pltpu.CompilerParams(vmem_limit_bytes=1024 * 1024),
+    )(*outs)
     return outs[0][None], outs[1][None], outs[2][None], outs[3][None], outs[4]
 
 

time: 54.5 us -> 48 us (0.88)
  local copies, waits for them, and re-layouts: 4.94 us -> 0 us
  Pallas kernels: 48.8 us -> 47.2 us
    unnamed x13 -> x0, local copies, waits for them, and re-layouts: 4.94 us -> none
    pallas_call x1 -> x2, Pallas kernels: 48.8 us -> 47.2 us  [the longest x1 45.7 us: per_device(): pl.pallas_call(functools.partial(kernel, sp, chips), out_shape=[pltpu.VME...]
where the time goes in v2:
time: 48 us; the launch traced here: 47.8 us
  Pallas kernels  47.2 us (98%)
  between operations  0.64 us (1%)
    pallas_call x1, Pallas kernels, per_device(): pl.pallas_call(functools.partial(kernel, sp, chips), out_shape=[pltpu.VME...  45.7 us
    pallas_call x1, Pallas kernels, per_device(): pl.pallas_call(write_out, out_shape=shapes, in_specs=[pl.BlockSpec(memory...  1.44 us

profile of v2, /device:TPU:0, one launch (start us, length us, event | category | flops | bytes accessed | tf_op | source)
XLA Modules:
  0.0 47.8 jit_solution(2351011007370208678)
XLA Ops:
  0.6 45.7 %shard_map.110 = (bf16[128,1024]{1,0:T(8,128)(2,1)S(1)}, bf16[128,1024]{1,0:T(8,128)(2,1)S(1)}, bf16[128,1024]{1,0:T(8,128)(2,1)S(1)}, bf16[128,2048]{1,0:T(8,128)(2,1)S(1)}, f32[256,1024]{1,0:T(8,128)S(1)}) custom-call(bf16[128,2048]{1,0:T(8,128)(2,1)} %bitcast.10, bf16[128,1024]{1,0:T(8,128)(2,1)} %bitcast.11, bf16[128,1024]{1,0:T(8,128)(2,1)} %bitcast.12, ...), custom_call_target="tpu_custom_call" | custom-call | tf_op jit(solution)/shard_map/pallas_call | solution.py:492
  46.4 1.4 %shard_map.111 = (bf16[128,1024]{1,0:T(8,128)(2,1)}, bf16[128,1024]{1,0:T(8,128)(2,1)}, bf16[128,1024]{1,0:T(8,128)(2,1)}, bf16[128,2048]{1,0:T(8,128)(2,1)}, f32[256,1024]{1,0:T(8,128)}) custom-call(bf16[128,1024]{1,0:T(8,128)(2,1)S(1)} %get-tuple-element.15.refs_0_, bf16[128,1024]{1,0:T(8,128)(2,1)S(1)} %get-tuple-element.16.refs_1_, ...), custom_call_target="tpu_custom_call" | custom-call | tf_op jit(solution)/shard_map/pallas_call | solution.py:522

commit v3 on v2

--- a/solution.py
+++ b/solution.py
@@ -41,7 +41,7 @@
     dqf_s, dqb_s, dkf_s, dkb_s, dv_s,
     sf_s, sb_s, ee_s,
     fin, bin_, fout, bout,
-    xin, xt, vgs, wpair, gin, gout,
+    xin, xt, vgs, wpair, gout,
     half_out, half_in, part, gfin, gbin, gfout, gbout,
     s_f, r_f, s_b, r_b, s_x, r_x, s_v, r_v, s_w, r_w, s_g, r_g, s_h, r_h,
     s_gf, r_gf, s_gb, r_gb, loc,
@@ -154,7 +154,7 @@
         zero = jnp.zeros_like(a)
         return jnp.concatenate([jnp.where(left, a, zero), jnp.where(left, zero, a)], axis=0)
 
-    def phase_a(p, carry):
+    def phase_a(p):
         sl = lanes(p)
         gate = g_ref[:, sl]
         run = nn(tril, gate)
@@ -190,19 +190,29 @@
         sb_s[p] = sb
         ee_s[p] = jnp.exp(tn(gate, ones_c))
 
+    group = 2 if pairs % 2 == 0 else 1
+
+    def phase_a_loop(i, carry):
+        for n in range(group):
+            phase_a(i * group + n)
+
         @pl.when(first)
         def _():
-            fout[p] = sf.astype(BF)
-            copy_f(p).start()
+            for n in range(group):
+                p = i * group + n
+                fout[p] = sf_s[p].astype(BF)
+                copy_f(p).start()
 
         @pl.when(last)
         def _():
-            bout[p] = sb.astype(BF)
-            copy_b(p).start()
+            for n in range(group):
+                p = i * group + n
+                bout[p] = sb_s[p].astype(BF)
+                copy_b(p).start()
 
         return carry
 
-    lax.fori_loop(0, pairs, phase_a, 0)
+    lax.fori_loop(0, pairs // group, phase_a_loop, 0)
 
     def forward_step(p):
         copy_f(p).wait_recv()
@@ -231,7 +241,7 @@
         def _():
             forward_step(p)
 
-    def phase_b(p, carry):
+    def phase_b(p):
         sl = lanes(p)
         qf2 = stack(qf_s[:, sl])
         qb2 = stack(qb_s[:, sl])
@@ -248,18 +258,24 @@
         dqf_s[:, sl] = nn(jnp.concatenate([dlow[:tokens], dlow[tokens:]], axis=1), stack(kf))
         dqb_s[:, sl] = nn(jnp.concatenate([dup[:tokens], dup[tokens:]], axis=1), stack(kb))
 
-        @pl.when(jnp.logical_and(lower_half, z > 0))
-        def _():
-            forward_step(p)
-
-        @pl.when(jnp.logical_and(jnp.logical_not(lower_half), z < sp - 1))
-        def _():
-            backward_step(p)
-
-        second_step(p - lag, jnp.logical_and(inner, p >= lag))
+    def phase_b_loop(i, carry):
+        for n in range(group):
+            phase_b(i * group + n)
+        for n in range(group):
+            p = i * group + n
+
+            @pl.when(jnp.logical_and(lower_half, z > 0))
+            def _():
+                forward_step(p)
+
+            @pl.when(jnp.logical_and(jnp.logical_not(lower_half), z < sp - 1))
+            def _():
+                backward_step(p)
+
+            second_step(p - lag, jnp.logical_and(inner, p >= lag))
         return carry
 
-    lax.fori_loop(0, pairs, phase_b, 0)
+    lax.fori_loop(0, pairs // group, phase_b_loop, 0)
 
     def received(p):
         f_in = fin[p].astype(F32)
@@ -268,7 +284,7 @@
         gf = jnp.where(diag, b_roll, 0.0).astype(BF)
         return f_in, b_roll, gb, gf
 
-    def phase_v(p, carry):
+    def phase_v(p):
         sl = lanes(p)
         second_step(p, jnp.logical_not(inner))
         second_step(p + lag, jnp.logical_and(inner, p < pairs - lag))
@@ -277,9 +293,15 @@
         vgs[mine(chip), sl] = dv.astype(BF)
         for j in range(1, chips):
             copy_v(j, p).start()
+
+    def phase_v_loop(p, carry):
+        @pl.when(jnp.logical_or(inner, p < lag))
+        def _():
+            phase_v(p)
+
         return carry
 
-    lax.fori_loop(0, pairs, phase_v, 0)
+    lax.fori_loop(0, pairs, phase_v_loop, 0)
 
     def phase_c(p):
         sl = lanes(p)
@@ -382,7 +404,9 @@
             copy_gb(p).start()
 
     def sum_step(p, lower, upper):
-        within = jnp.logical_and(inner, jnp.logical_and(p >= 0, p < pairs))
+        within = inner
+        if not isinstance(p, int):
+            within = jnp.logical_and(inner, jnp.logical_and(p >= 0, p < pairs))
 
         @pl.when(jnp.logical_and(within, lower_half))
         def _():
@@ -393,17 +417,25 @@
             upper(p)
 
     def pipeline(i, carry):
+        @pl.when(jnp.logical_and(jnp.logical_not(inner), i < pairs - lag))
+        def _():
+            phase_v(i + lag)
+
         @pl.when(i < pairs)
         def _():
             make_term(i)
+
+        @pl.when(jnp.logical_and(i >= 1, i <= pairs))
+        def _():
+            join(i - 1)
+
+        sum_step(i - 2, sum_forward, sum_backward)
+        sum_step(i - 4, sum_backward, sum_forward)
+
+        @pl.when(i < pairs)
+        def _():
             phase_c(i)
 
-        @pl.when(jnp.logical_and(i >= 1, i <= pairs))
-        def _():
-            join(i - 1)
-
-        sum_step(i - 3, sum_forward, sum_backward)
-        sum_step(i - 5, sum_backward, sum_forward)
         return carry
 
     lax.fori_loop(0, pairs + 1, pipeline, 0)
@@ -411,21 +443,28 @@
     def copy_g(j):
         other, idx = peer(j)
         return pltpu.make_async_remote_copy(
-            gout.at[mine(other)], gin.at[chip], s_g.at[j], r_g.at[j], device_id={"dp": idx})
+            gout.at[mine(other)], gi_ref.at[:, chip_cols(chip)], s_g.at[j], r_g.at[j], device_id={"dp": idx})
 
     def project(j):
         other, _ = peer(j)
         gout[mine(other), :] = nt(vgs[mine(other), :], wpair[...]).astype(BF)
 
-    for j in range(1, chips):
+    def project_to(j):
         project(j)
-        copy_g(j).start()
+        if j:
+            copy_g(j).start()
+
+    sum_step(pairs - 1, sum_forward, sum_backward)
+    project_to(1)
+    sum_step(pairs - 3, sum_backward, sum_forward)
+    for j in range(2, chips - 1):
+        project_to(j)
+    sum_step(pairs - 2, sum_backward, sum_forward)
+    project_to(chips - 1)
+    sum_step(pairs - 1, sum_backward, sum_forward)
     project(0)
     gi_ref[:, chip_cols(chip)] = gout[mine(chip), :]
 
-
-    lax.fori_loop(pairs + 1, pairs + 5, pipeline, 0)
-
     def finish(p, carry):
         @pl.when(first)
         def _():
@@ -442,9 +481,6 @@
 
     for j in range(1, chips):
         copy_g(j).wait()
-    for j in range(1, chips):
-        other, _ = peer(j)
-        gi_ref[:, chip_cols(other)] = gin[other]
 
     @pl.when(z < sp - 1)
     def _():
@@ -505,7 +541,6 @@
             pltpu.VMEM((2 * rows, chips * tokens), BF),
             pltpu.VMEM((chips * tokens, width), BF),
             pltpu.VMEM((2 * rows, width), BF),
-            pltpu.VMEM((chips, tokens, 2 * rows), BF),
             pltpu.VMEM((chips * tokens, 2 * rows), BF),
             piece(BF), piece(BF), piece(F32), piece(BF), piece(BF), piece(BF), piece(BF),
         ]

time: 48 us -> 46.8 us (0.975)
  Pallas kernels: 47.2 us -> 46.1 us
    pallas_call x1, Pallas kernels: 45.7 us -> 44.6 us  [per_device(): pl.pallas_call(functools.partial(kernel, sp, chips), out_shape=[pltpu.VME...]
where the time goes in v3:
time: 46.8 us; the launch traced here: 46.7 us
  Pallas kernels  46.1 us (99%)
  between operations  0.64 us (1%)
    pallas_call x1, Pallas kernels, per_device(): pl.pallas_call(functools.partial(kernel, sp, chips), out_shape=[pltpu.VME...  44.6 us
    pallas_call x1, Pallas kernels, per_device(): pl.pallas_call(write_out, out_shape=shapes, in_specs=[pl.BlockSpec(memory...  1.44 us

profile of v3, /device:TPU:0, one launch (start us, length us, event | category | flops | bytes accessed | tf_op | source)
XLA Modules:
  0.0 46.7 jit_solution(16224409181722011232)
XLA Ops:
  0.6 44.6 %shard_map.110 = (bf16[128,1024]{1,0:T(8,128)(2,1)S(1)}, bf16[128,1024]{1,0:T(8,128)(2,1)S(1)}, bf16[128,1024]{1,0:T(8,128)(2,1)S(1)}, bf16[128,2048]{1,0:T(8,128)(2,1)S(1)}, f32[256,1024]{1,0:T(8,128)S(1)}) custom-call(bf16[128,2048]{1,0:T(8,128)(2,1)} %bitcast.10, bf16[128,1024]{1,0:T(8,128)(2,1)} %bitcast.11, bf16[128,1024]{1,0:T(8,128)(2,1)} %bitcast.12, ...), custom_call_target="tpu_custom_call" | custom-call | tf_op jit(solution)/shard_map/pallas_call | solution.py:528
  45.3 1.4 %shard_map.111 = (bf16[128,1024]{1,0:T(8,128)(2,1)}, bf16[128,1024]{1,0:T(8,128)(2,1)}, bf16[128,1024]{1,0:T(8,128)(2,1)}, bf16[128,2048]{1,0:T(8,128)(2,1)}, f32[256,1024]{1,0:T(8,128)}) custom-call(bf16[128,1024]{1,0:T(8,128)(2,1)S(1)} %get-tuple-element.15.refs_0_, bf16[128,1024]{1,0:T(8,128)(2,1)S(1)} %get-tuple-element.16.refs_1_, ...), custom_call_target="tpu_custom_call" | custom-call | tf_op jit(solution)/shard_map/pallas_call | solution.py:557
